TPU v7x, 32 devices: a whole 2x2x4 slice. The times are simulated.
32 devices in a mesh: sp: 4 (over z), dp: 8 (over y, x, core).
Axes of the slice: x: 2, y: 2, z: 4, core: 2. Of those that a mesh axis runs over, the one named last changes fastest.
Arguments:
- queries: bfloat16 [8, 512, 1024], P('dp', 'sp'), may hold values from -6 to 6
- key_rows: bfloat16 [8, 512, 1024], P('dp', 'sp'), may hold values from -6 to 6
- values: bfloat16 [8, 512, 2048], P('dp', 'sp'), may hold values from -6 to 6
- out_gate: bfloat16 [8, 512, 2048], P('dp', 'sp'), may hold values from -6 to 6
- input_gate: bfloat16 [8, 4, 512], P('dp', None, 'sp'), may hold values from -6 to 205
- forget_gate: bfloat16 [8, 4, 512], P('dp', None, 'sp'), may hold values from 0.5 to 13
- out_weight: bfloat16 [2048, 2048], P(None, 'dp'), may hold values from -0.125 to 0.125
Outputs:
- layer_out: bfloat16 [8, 512, 2048], P('dp', 'sp')
All inputs are finite; a program needn't handle non-finite values.
Results may differ from a plain program's by a relative error of at most 0.0057.
Values may be sent and summed in bfloat16 or wider, within the bound.
A program may use at most 64 MiB of HBM per device.

v0:
```python
import jax
import jax.numpy as jnp
from jax import lax
from jax.sharding import PartitionSpec as P

BLOCK = 128


def memory_cell(query_rows, key_in, value_rows, input_log, forget_log):
    block_count = query_rows.shape[0] // BLOCK
    key_width = query_rows.shape[1]
    value_width = value_rows.shape[1]
    key_scale = key_width ** (-0.5)
    causal = lax.broadcasted_iota(jnp.int32, (BLOCK, BLOCK), 0) >= lax.broadcasted_iota(
        jnp.int32, (BLOCK, BLOCK), 1
    )
    highest = lax.Precision.HIGHEST

    def block_step(state_in, inputs):
        memory, normer, stabil = state_in
        query_part, key_part, value_part, gain_part, decay_part = inputs
        query_part = query_part.astype(jnp.float32)
        key_part = key_part.astype(jnp.float32) * key_scale
        value_part = value_part.astype(jnp.float32)
        running = jnp.cumsum(decay_part)
        log_weight = running[:, None] - running[None, :] + gain_part[None, :]
        log_weight = jnp.where(causal, log_weight, -jnp.inf)
        carried_log = running + stabil
        row_top = jnp.maximum(carried_log, jnp.max(log_weight, axis=1))
        scores = jnp.dot(query_part, key_part.T, precision=highest) * jnp.exp(
            log_weight - row_top[:, None]
        )
        carried = jnp.exp(carried_log - row_top)
        numerator = jnp.dot(scores, value_part, precision=highest) + carried[:, None] * jnp.dot(
            query_part, memory, precision=highest
        )
        denominator = jnp.sum(scores, axis=1) + carried * jnp.dot(
            query_part, normer, precision=highest
        )
        output = numerator / jnp.maximum(jnp.abs(denominator), 1.0)[:, None]
        block_end = running[-1]
        weight_log = block_end - running + gain_part
        new_top = jnp.maximum(block_end + stabil, jnp.max(weight_log))
        weights = jnp.exp(weight_log - new_top)
        retain = jnp.exp(block_end + stabil - new_top)
        memory = retain * memory + jnp.dot(
            (key_part * weights[:, None]).T, value_part, precision=highest
        )
        normer = retain * normer + jnp.dot(weights, key_part, precision=highest)
        return ((memory, normer, new_top), output)

    start_state = (
        jnp.zeros((key_width, value_width), jnp.float32),
        jnp.zeros((key_width,), jnp.float32),
        jnp.zeros((), jnp.float32),
    )
    blocks = tuple(
        (
            source.reshape((block_count, BLOCK) + source.shape[1:])
            for source in (query_rows, key_in, value_rows, input_log, forget_log)
        )
    )
    _, outputs = lax.scan(block_step, start_state, blocks)
    return outputs.reshape(block_count * BLOCK, value_width)


def body(queries, key_rows, values, out_gate, input_gate, forget_gate, out_weight):
    group_count = lax.axis_size("sp")
    token_count = queries.shape[1]
    head_count = input_gate.shape[1]
    copies = group_count // head_count
    head_key = queries.shape[2] // head_count
    slice_width = values.shape[2] // group_count

    def spread(source):
        widened = jnp.broadcast_to(
            source[0].reshape(token_count, head_count, 1, head_key),
            (token_count, head_count, copies, head_key),
        )
        return widened.reshape(token_count, group_count, head_key)

    def spread_gate(source):
        return jnp.repeat(source[0].T, copies, axis=1)

    query_all, key_all = (
        lax.all_to_all(spread(queries), "sp", split_axis=1, concat_axis=0, tiled=True),
        lax.all_to_all(spread(key_rows), "sp", split_axis=1, concat_axis=0, tiled=True),
    )
    value_all, input_all, forget_all = (
        lax.all_to_all(
            values[0].reshape(token_count, group_count, slice_width),
            "sp",
            split_axis=1,
            concat_axis=0,
            tiled=True,
        ),
        lax.all_to_all(spread_gate(input_gate), "sp", split_axis=1, concat_axis=0, tiled=True),
        lax.all_to_all(spread_gate(forget_gate), "sp", split_axis=1, concat_axis=0, tiled=True),
    )
    output = memory_cell(
        query_all[:, 0],
        key_all[:, 0],
        value_all[:, 0],
        input_all[:, 0].astype(jnp.float32),
        jax.nn.log_sigmoid(forget_all[:, 0].astype(jnp.float32)),
    )
    hidden = output.astype(jnp.bfloat16)
    token_rows = lax.all_to_all(hidden, "sp", split_axis=0, concat_axis=1, tiled=True)
    gated_rows = (
        token_rows.astype(jnp.float32) * jax.nn.sigmoid(out_gate[0].astype(jnp.float32))
    ).astype(jnp.bfloat16)
    projected = jnp.dot(
        gated_rows,
        lax.all_gather(out_weight, "dp", axis=1, tiled=True),
        preferred_element_type=jnp.float32,
    )
    return projected.astype(jnp.bfloat16)[None]


def solution(mesh):
    return jax.shard_map(
        body,
        mesh=mesh,
        in_specs=(
            P("dp", "sp", None),
            P("dp", "sp", None),
            P("dp", "sp", None),
            P("dp", "sp", None),
            P("dp", None, "sp"),
            P("dp", None, "sp"),
            P(None, "dp"),
        ),
        out_specs=P("dp", "sp", None),
        check_vma=False,
    )
```

profile of v0, /device:TPU:0, one launch (start us, length us, event | category | flops | bytes accessed | tf_op | source)
XLA Modules:
  0.0 121.6 jit_solution(9997319030571958665)
XLA Ops:
  6.5 0.7 all-gather.2.cloned.1.call-update
  7.3 1.3 %copy.28 = bf16[128,4,1]{0,2,1:T(2,128)(2,1)} copy(bf16[128,4,1]{0,1,2:T(4,128)(2,1)} %bitcast.152) | data formatting | bytes 2048 | tf_op jit(solution)/shard_map/all_to_all | solution.py:98
  8.5 6.3 %all-to-all-start = ((bf16[128,4,1]{0,2,1:T(2,128)(2,1)}), bf16[128,4,1]{0,2,1:T(2,128)(2,1)S(1)}, u32[]{:S(2)}, u32[]{:S(2)}) async-start(bf16[128,4,1]{0,2,1:T(2,128)(2,1)} %copy.28), calls=%async_computation | async-start | bytes 4096 | tf_op jit(solution)/shard_map/all_to_all | solution.py:98
  14.9 1.3 %copy.29 = bf16[128,4,1]{0,2,1:T(2,128)(2,1)} copy(bf16[128,4,1]{0,1,2:T(4,128)(2,1)} %bitcast.153) | data formatting | bytes 2048 | tf_op jit(solution)/shard_map/all_to_all | solution.py:97
  16.1 4.2 %all-to-all-done = bf16[128,4,1]{0,2,1:T(2,128)(2,1)S(1)} async-done(((bf16[128,4,1]{0,2,1:T(2,128)(2,1)}), bf16[128,4,1]{0,2,1:T(2,128)(2,1)S(1)}, u32[]{:S(2)}, u32[]{:S(2)}) %all-to-all-start) | async-done | bytes 1056 | tf_op jit(solution)/shard_map/all_to_all | solution.py:98
  20.4 3.2 %all-to-all-start.1 = ((bf16[128,4,1]{0,2,1:T(2,128)(2,1)}), bf16[128,4,1]{0,2,1:T(2,128)(2,1)S(1)}, u32[]{:S(2)}, u32[]{:S(2)}) async-start(bf16[128,4,1]{0,2,1:T(2,128)(2,1)} %copy.29), calls=%async_computation.1 | async-start | bytes 4096 | tf_op jit(solution)/shard_map/all_to_all | solution.py:97
  23.6 1.8 %copy.30 = bf16[1,128,1024]{1,2,0:T(8,128)(2,1)} copy(bf16[1,128,1024]{2,1,0:T(8,128)(2,1)} %param.10) | data formatting | bytes 524288 | tf_op args[1]
  25.4 3.6 %all-to-all-done.1 = bf16[128,4,1]{0,2,1:T(2,128)(2,1)S(1)} async-done(((bf16[128,4,1]{0,2,1:T(2,128)(2,1)}), bf16[128,4,1]{0,2,1:T(2,128)(2,1)S(1)}, u32[]{:S(2)}, u32[]{:S(2)}) %all-to-all-start.1) | async-done | bytes 1056 | tf_op jit(solution)/shard_map/all_to_all | solution.py:97
  29.0 3.4 %all-to-all-start.2 = ((bf16[128,4,256]{0,2,1:T(8,128)(2,1)}), bf16[128,4,256]{0,2,1:T(8,128)(2,1)S(1)}, u32[]{:S(2)}, u32[]{:S(2)}) async-start(bf16[128,4,256]{0,2,1:T(8,128)(2,1)} %bitcast.11), calls=%async_computation.2 | async-start | bytes 524288 | tf_op jit(solution)/shard_map/all_to_all | solution.py:87
  32.4 1.8 %copy.32 = bf16[1,128,1024]{1,2,0:T(8,128)(2,1)} copy(bf16[1,128,1024]{2,1,0:T(8,128)(2,1)} %param.9) | data formatting | bytes 524288 | tf_op args[0]
  34.2 4.9 %all-to-all-done.2 = bf16[128,4,256]{0,2,1:T(8,128)(2,1)S(1)} async-done(((bf16[128,4,256]{0,2,1:T(8,128)(2,1)}), bf16[128,4,256]{0,2,1:T(8,128)(2,1)S(1)}, u32[]{:S(2)}, u32[]{:S(2)}) %all-to-all-start.2) | async-done | bytes 262176 | tf_op jit(solution)/shard_map/all_to_all | solution.py:87
  39.1 3.4 %all-to-all-start.4 = ((bf16[128,4,256]{0,2,1:T(8,128)(2,1)}), bf16[128,4,256]{0,2,1:T(8,128)(2,1)S(1)}, u32[]{:S(2)}, u32[]{:S(2)}) async-start(bf16[128,4,256]{0,2,1:T(8,128)(2,1)} %bitcast.19), calls=%async_computation.4 | async-start | bytes 524288 | tf_op jit(solution)/shard_map/all_to_all | solution.py:86
  42.6 2.1 %copy.31 = bf16[1,128,2048]{1,2,0:T(8,128)(2,1)} copy(bf16[1,128,2048]{2,1,0:T(8,128)(2,1)} %param.11) | data formatting | bytes 1048576 | tf_op args[2]
  44.7 4.7 %all-to-all-done.4 = bf16[128,4,256]{0,2,1:T(8,128)(2,1)S(1)} async-done(((bf16[128,4,256]{0,2,1:T(8,128)(2,1)}), bf16[128,4,256]{0,2,1:T(8,128)(2,1)S(1)}, u32[]{:S(2)}, u32[]{:S(2)}) %all-to-all-start.4) | async-done | bytes 262176 | tf_op jit(solution)/shard_map/all_to_all | solution.py:86
  49.4 3.5 %all-to-all-start.3 = ((bf16[128,4,512]{0,2,1:T(8,128)(2,1)}), bf16[128,4,512]{0,2,1:T(8,128)(2,1)S(1)}, u32[]{:S(2)}, u32[]{:S(2)}) async-start(bf16[128,4,512]{0,2,1:T(8,128)(2,1)} %bitcast.15), calls=%async_computation.3 | async-start | bytes 1048576 | tf_op jit(solution)/shard_map/all_to_all | solution.py:90
  52.9 10.2 %all-to-all-done.3 = bf16[128,4,512]{0,2,1:T(8,128)(2,1)S(1)} async-done(((bf16[128,4,512]{0,2,1:T(8,128)(2,1)}), bf16[128,4,512]{0,2,1:T(8,128)(2,1)S(1)}, u32[]{:S(2)}, u32[]{:S(2)}) %all-to-all-start.3) | async-done | bytes 524320 | tf_op jit(solution)/shard_map/all_to_all | solution.py:90
  63.1 32.2 %while.17 = (s32[]{:T(128)}, f32[256,512]{1,0:T(8,128)S(1)}, f32[256]{0:T(256)S(1)}, f32[]{:T(128)}, bf16[4,128,512]{1,2,0:T(8,128)(2,1)}, /*index=5*/f32[4,128]...) while((s32[]{:T(128)}, f32[256,512]{1,0:T(8,128)S(1)}, ...), condition=%wide.region_5.6_spmd.clone, body=%wide.region_0.5_spmd.clone.sunk | while | flops 555633152 | bytes 3825425 | solution.py:63
  64.0 0.8 subtract_reduce_fusion.2
  64.7 1.3 %fusion.87 = (f32[]{:T(128)}, f32[128]{0:T(128)S(1)}) fusion(f32[128]{0:T(128)S(1)} %get-tuple-element.231, f32[]{:T(128)} %bitcast.142, f32[4,128]{1,0:T(4,128)S(1)} %get-tuple-element.274, s32[]{:T(128)} %get-tuple-element.255), kind=kLoop, calls=%fused_computation.63.clone.1 | loop fusion | flops 383 | bytes 1548 | tf_op jit(solution)/shard_map/while/body/eval_jaxpr/reduce_max | solution.py:43
  67.9 0.7 subtract_exponential_fusion.2
  72.0 0.8 subtract_reduce_fusion.2
  72.8 1.3 %fusion.87 = (f32[]{:T(128)}, f32[128]{0:T(128)S(1)}) fusion(f32[128]{0:T(128)S(1)} %get-tuple-element.231, f32[]{:T(128)} %bitcast.142, f32[4,128]{1,0:T(4,128)S(1)} %get-tuple-element.274, s32[]{:T(128)} %get-tuple-element.255), kind=kLoop, calls=%fused_computation.63.clone.1 | loop fusion | flops 383 | bytes 1548 | tf_op jit(solution)/shard_map/while/body/eval_jaxpr/reduce_max | solution.py:43
  76.0 0.7 subtract_exponential_fusion.2
  80.0 0.8 subtract_reduce_fusion.2
  80.8 1.3 %fusion.87 = (f32[]{:T(128)}, f32[128]{0:T(128)S(1)}) fusion(f32[128]{0:T(128)S(1)} %get-tuple-element.231, f32[]{:T(128)} %bitcast.142, f32[4,128]{1,0:T(4,128)S(1)} %get-tuple-element.274, s32[]{:T(128)} %get-tuple-element.255), kind=kLoop, calls=%fused_computation.63.clone.1 | loop fusion | flops 383 | bytes 1548 | tf_op jit(solution)/shard_map/while/body/eval_jaxpr/reduce_max | solution.py:43
  84.0 0.7 subtract_exponential_fusion.2
  88.1 0.8 subtract_reduce_fusion.2
  88.9 1.3 %fusion.87 = (f32[]{:T(128)}, f32[128]{0:T(128)S(1)}) fusion(f32[128]{0:T(128)S(1)} %get-tuple-element.231, f32[]{:T(128)} %bitcast.142, f32[4,128]{1,0:T(4,128)S(1)} %get-tuple-element.274, s32[]{:T(128)} %get-tuple-element.255), kind=kLoop, calls=%fused_computation.63.clone.1 | loop fusion | flops 383 | bytes 1548 | tf_op jit(solution)/shard_map/while/body/eval_jaxpr/reduce_max | solution.py:43
  92.0 0.7 subtract_exponential_fusion.2
  95.2 3.5 %all-to-all-start.5 = ((bf16[4,128,512]{1,2,0:T(8,128)(2,1)}), bf16[4,128,512]{1,2,0:T(8,128)(2,1)S(1)}, u32[]{:S(2)}, u32[]{:S(2)}) async-start(bf16[4,128,512]{1,2,0:T(8,128)(2,1)} %get-tuple-element.62), calls=%async_computation.5 | async-start | bytes 1048576 | tf_op jit(solution)/shard_map/all_to_all | solution.py:108
  99.0 10.0 %all-to-all-done.5 = bf16[4,128,512]{1,2,0:T(8,128)(2,1)S(1)} async-done(((bf16[4,128,512]{1,2,0:T(8,128)(2,1)}), bf16[4,128,512]{1,2,0:T(8,128)(2,1)S(1)}, u32[]{:S(2)}, u32[]{:S(2)}) %all-to-all-start.5) | async-done | bytes 524320 | tf_op jit(solution)/shard_map/all_to_all | solution.py:108
  109.3 5.5 %fusion.49 = bf16[1,128,2048]{2,1,0:T(8,128)(2,1)} fusion(bf16[128,2048]{0,1:T(8,128)(2,1)S(1)} %fusion.50, bf16[2048,2048]{1,0:T(8,128)(2,1)} %all-gather.2.cloned.1.call-done), kind=kOutput, calls=%fused_computation.65 | convolution fusion | flops 1074003968 | bytes 9437184 | tf_op jit(solution)/shard_map/dot_general | solution.py:112
  (76 shorter events, 15.7 us)
Async XLA Ops:
  6.5 102.8 %all-gather.2.cloned.1.call-start = ((), (), s32[]{:S(2)}) async-start(), calls=%async_computation.6 | async-start | bytes 9437184 | tf_op jit(solution)/shard_map/all_gather | solution.py:114
  8.5 11.8 %all-to-all-start = ((bf16[128,4,1]{0,2,1:T(2,128)(2,1)}), bf16[128,4,1]{0,2,1:T(2,128)(2,1)S(1)}, u32[]{:S(2)}, u32[]{:S(2)}) async-start(bf16[128,4,1]{0,2,1:T(2,128)(2,1)} %copy.28), calls=%async_computation | async-start | bytes 4096 | tf_op jit(solution)/shard_map/all_to_all | solution.py:98
  20.4 8.6 %all-to-all-start.1 = ((bf16[128,4,1]{0,2,1:T(2,128)(2,1)}), bf16[128,4,1]{0,2,1:T(2,128)(2,1)S(1)}, u32[]{:S(2)}, u32[]{:S(2)}) async-start(bf16[128,4,1]{0,2,1:T(2,128)(2,1)} %copy.29), calls=%async_computation.1 | async-start | bytes 4096 | tf_op jit(solution)/shard_map/all_to_all | solution.py:97
  29.0 10.2 %all-to-all-start.2 = ((bf16[128,4,256]{0,2,1:T(8,128)(2,1)}), bf16[128,4,256]{0,2,1:T(8,128)(2,1)S(1)}, u32[]{:S(2)}, u32[]{:S(2)}) async-start(bf16[128,4,256]{0,2,1:T(8,128)(2,1)} %bitcast.11), calls=%async_computation.2 | async-start | bytes 524288 | tf_op jit(solution)/shard_map/all_to_all | solution.py:87
  39.1 10.2 %all-to-all-start.4 = ((bf16[128,4,256]{0,2,1:T(8,128)(2,1)}), bf16[128,4,256]{0,2,1:T(8,128)(2,1)S(1)}, u32[]{:S(2)}, u32[]{:S(2)}) async-start(bf16[128,4,256]{0,2,1:T(8,128)(2,1)} %bitcast.19), calls=%async_computation.4 | async-start | bytes 524288 | tf_op jit(solution)/shard_map/all_to_all | solution.py:86
  49.4 13.7 %all-to-all-start.3 = ((bf16[128,4,512]{0,2,1:T(8,128)(2,1)}), bf16[128,4,512]{0,2,1:T(8,128)(2,1)S(1)}, u32[]{:S(2)}, u32[]{:S(2)}) async-start(bf16[128,4,512]{0,2,1:T(8,128)(2,1)} %bitcast.15), calls=%async_computation.3 | async-start | bytes 1048576 | tf_op jit(solution)/shard_map/all_to_all | solution.py:90
  63.1 35.7 %copy-start = (bf16[1,128,2048]{2,1,0:T(8,128)(2,1)S(1)}, bf16[1,128,2048]{2,1,0:T(8,128)(2,1)}, u32[]{:S(2)}) copy-start(bf16[1,128,2048]{2,1,0:T(8,128)(2,1)} %param.12) | copy-start | bytes 1572868
  95.2 13.7 %all-to-all-start.5 = ((bf16[4,128,512]{1,2,0:T(8,128)(2,1)}), bf16[4,128,512]{1,2,0:T(8,128)(2,1)S(1)}, u32[]{:S(2)}, u32[]{:S(2)}) async-start(bf16[4,128,512]{1,2,0:T(8,128)(2,1)} %get-tuple-element.62), calls=%async_computation.5 | async-start | bytes 1048576 | tf_op jit(solution)/shard_map/all_to_all | solution.py:108
Sparse Core Ops, SparseCore 0:
  9.2 58.5 all-gather.1
where the time goes:
time: 122 us
  waiting for transfers between devices  38.3 us (31%)
  starting transfers between devices  23.4 us (19%)
  local copies, waits for them, and re-layouts  15 us (12%)
  between operations  13.5 us (11%)
  matrix products  12.9 us (11%)
  other arithmetic  12.7 us (10%)
  loops' own time  5.83 us (5%)
    all_to_all x1, waiting for transfers between devices, body(): lax.all_to_all(values[0].reshape(token_count, group_count, slice_width),...  10.2 us
    all_to_all x1, waiting for transfers between devices, body(): lax.all_to_all(hidden, 'sp', split_axis=0, concat_axis=1, tiled=True)  9.97 us
    all_to_all x1, starting transfers between devices, body(): lax.all_to_all(spread_gate(forget_gate), 'sp', split_axis=1, concat_axis=...  6.35 us
    unnamed x6, local copies, waits for them, and re-layouts  6 us
    another operation x1, loops' own time, memory_cell(): _, outputs = lax.scan(block_step, start_state, blocks)  5.83 us
    dot_general x1, matrix products, body(): jnp.dot(gated_rows, lax.all_gather(out_weight, 'dp', axis=1, tiled=True),...  5.46 us
    reduce_max x4, other arithmetic, block_step(): new_top = jnp.maximum(block_end + stabil, jnp.max(weight_log))  5.38 us
    all_to_all x1, waiting for transfers between devices, body(): lax.all_to_all(spread(key_rows), 'sp', split_axis=1, concat_axis=0, tiled...  4.92 us
  transfers between devices with their start and end apart: 7, of which 6 were waited for; matrix products, arithmetic and copies ran while one was open for 29% of the time, Pallas kernels for 0%

commit v1 on v0

--- a/solution.py
+++ b/solution.py
@@ -4,6 +4,29 @@
 from jax.sharding import PartitionSpec as P
 
 BLOCK = 128
+
+
+def split_up(x, dim, devices):
+    dims = x.shape
+    blocks = x.reshape(*dims[:dim], devices, dims[dim] // devices, *dims[dim + 1 :])
+    return jnp.moveaxis(blocks, dim, 0)
+
+
+def in_order(blocks, dim):
+    blocks = jnp.moveaxis(blocks, 0, dim)
+    shape = blocks.shape
+    return blocks.reshape(*shape[:dim], shape[dim] * shape[dim + 1], *shape[dim + 2 :])
+
+
+def sent_to_each(value, axis, split_dim, concat_dim):
+    count, mine = (lax.axis_size(axis), lax.axis_index(axis))
+    blocks = split_up(value, split_dim, count)
+    outs = [blocks[mine]]
+    for step in range(1, count):
+        sent = blocks[(mine + step) % count]
+        outs.append(lax.ppermute(sent, axis, [(i, (i + step) % count) for i in range(count)]))
+    blocks = jnp.stack(outs)[(mine - jnp.arange(count)) % count]
+    return in_order(blocks, concat_dim)
 
 
 def memory_cell(query_rows, key_in, value_rows, input_log, forget_log):
@@ -95,7 +118,7 @@
             tiled=True,
         ),
         lax.all_to_all(spread_gate(input_gate), "sp", split_axis=1, concat_axis=0, tiled=True),
-        lax.all_to_all(spread_gate(forget_gate), "sp", split_axis=1, concat_axis=0, tiled=True),
+        sent_to_each(spread_gate(forget_gate), "sp", 1, 0),
     )
     output = memory_cell(
         query_all[:, 0],

time: 122 us -> 115 us (0.943)
  waiting for transfers between devices: 38.3 us -> 29.4 us
  starting transfers between devices: 23.4 us -> 25 us
    all_to_all x1, waiting for transfers between devices: 10.2 us -> 0.01 us  [body(): lax.all_to_all(values[0].reshape(token_count, group_count, slice_width),...]
    all_to_all x1 -> x0, starting transfers between devices: 6.35 us -> none  [body(): lax.all_to_all(spread_gate(forget_gate), 'sp', split_axis=1, concat_axis=...]
    ppermute x0 -> x3, waiting for transfers between devices: none -> 5.05 us  [sent_to_each(): lax.ppermute(sent, axis, [(i, (i + step) % count) for i in range(count)])]
    ppermute x0 -> x3, starting transfers between devices: none -> 4.86 us  [sent_to_each(): lax.ppermute(sent, axis, [(i, (i + step) % count) for i in range(count)])]
    all_to_all x1 -> x0, waiting for transfers between devices: 4.22 us -> none  [body(): lax.all_to_all(spread_gate(forget_gate), 'sp', split_axis=1, concat_axis=...]
    all_to_all x1, starting transfers between devices: 3.23 us -> 6.35 us  [body(): lax.all_to_all(spread_gate(input_gate), 'sp', split_axis=1, concat_axis=0...]
    all_to_all x1 -> x0, local copies, waits for them, and re-layouts: 1.26 us -> none  [body(): lax.all_to_all(spread_gate(forget_gate), 'sp', split_axis=1, concat_axis=...]
  transfers between devices with their start and end apart: 7 -> 9, of which waited for: 6 -> 7; matrix products, arithmetic and copies ran while one was open for 29% -> 30% of each run, Pallas kernels for 0% -> 0%
where the time goes in v1:
time: 115 us; the launch traced here: 114 us
  waiting for transfers between devices  29.4 us (26%)
  starting transfers between devices  25 us (22%)
  local copies, waits for them, and re-layouts  14.9 us (13%)
  between operations  13.6 us (12%)
  matrix products  12.9 us (11%)
  other arithmetic  12.3 us (11%)
  loops' own time  5.87 us (5%)
    all_to_all x1, waiting for transfers between devices, body(): lax.all_to_all(hidden, 'sp', split_axis=0, concat_axis=1, tiled=True)  9.97 us
    all_to_all x1, starting transfers between devices, body(): lax.all_to_all(spread_gate(input_gate), 'sp', split_axis=1, concat_axis=0...  6.35 us
    unnamed x6, local copies, waits for them, and re-layouts  5.96 us
    another operation x1, loops' own time, memory_cell(): _, outputs = lax.scan(block_step, start_state, blocks)  5.87 us
    dot_general x1, matrix products, body(): jnp.dot(gated_rows, lax.all_gather(out_weight, 'dp', axis=1, tiled=True),...  5.46 us
    reduce_max x4, other arithmetic, block_step(): new_top = jnp.maximum(block_end + stabil, jnp.max(weight_log))  5.23 us
    all_to_all x1, waiting for transfers between devices, body(): lax.all_to_all(spread(key_rows), 'sp', split_axis=1, concat_axis=0, tiled...  5.22 us
    ppermute x3, waiting for transfers between devices, sent_to_each(): lax.ppermute(sent, axis, [(i, (i + step) % count) for i in range(count)])  5.05 us
  transfers between devices with their start and end apart: 9, of which 7 were waited for; matrix products, arithmetic and copies ran while one was open for 30% of the time, Pallas kernels for 0%

profile of v1, /device:TPU:0, one launch (start us, length us, event | category | flops | bytes accessed | tf_op | source)
XLA Modules:
  0.0 113.9 jit_solution(518766541164611768)
XLA Ops:
  6.5 0.7 all-gather.2.cloned.1.call-update
  7.3 1.3 %copy.44 = bf16[128,4,1]{0,2,1:T(2,128)(2,1)} copy(bf16[128,4,1]{0,1,2:T(4,128)(2,1)} %bitcast.166) | data formatting | bytes 2048 | tf_op jit(solution)/shard_map/all_to_all | solution.py:120
  8.5 6.3 %all-to-all-start = ((bf16[128,4,1]{0,2,1:T(2,128)(2,1)}), bf16[128,4,1]{0,2,1:T(2,128)(2,1)S(1)}, u32[]{:S(2)}, u32[]{:S(2)}) async-start(bf16[128,4,1]{0,2,1:T(2,128)(2,1)} %copy.44), calls=%async_computation | async-start | bytes 4096 | tf_op jit(solution)/shard_map/all_to_all | solution.py:120
  14.9 1.8 %copy.45 = bf16[1,128,1024]{1,2,0:T(8,128)(2,1)} copy(bf16[1,128,1024]{2,1,0:T(8,128)(2,1)} %param.10) | data formatting | bytes 524288 | tf_op args[1]
  16.7 3.8 %all-to-all-done = bf16[128,4,1]{0,2,1:T(2,128)(2,1)S(1)} async-done(((bf16[128,4,1]{0,2,1:T(2,128)(2,1)}), bf16[128,4,1]{0,2,1:T(2,128)(2,1)S(1)}, u32[]{:S(2)}, u32[]{:S(2)}) %all-to-all-start) | async-done | bytes 1056 | tf_op jit(solution)/shard_map/all_to_all | solution.py:120
  20.4 3.4 %all-to-all-start.1 = ((bf16[128,4,256]{0,2,1:T(8,128)(2,1)}), bf16[128,4,256]{0,2,1:T(8,128)(2,1)S(1)}, u32[]{:S(2)}, u32[]{:S(2)}) async-start(bf16[128,4,256]{0,2,1:T(8,128)(2,1)} %bitcast.18), calls=%async_computation.1 | async-start | bytes 524288 | tf_op jit(solution)/shard_map/all_to_all | solution.py:110
  23.9 1.8 %copy.47 = bf16[1,128,1024]{1,2,0:T(8,128)(2,1)} copy(bf16[1,128,1024]{2,1,0:T(8,128)(2,1)} %param.9) | data formatting | bytes 524288 | tf_op args[0]
  25.7 5.2 %all-to-all-done.1 = bf16[128,4,256]{0,2,1:T(8,128)(2,1)S(1)} async-done(((bf16[128,4,256]{0,2,1:T(8,128)(2,1)}), bf16[128,4,256]{0,2,1:T(8,128)(2,1)S(1)}, u32[]{:S(2)}, u32[]{:S(2)}) %all-to-all-start.1) | async-done | bytes 262176 | tf_op jit(solution)/shard_map/all_to_all | solution.py:110
  30.9 3.4 %all-to-all-start.3 = ((bf16[128,4,256]{0,2,1:T(8,128)(2,1)}), bf16[128,4,256]{0,2,1:T(8,128)(2,1)S(1)}, u32[]{:S(2)}, u32[]{:S(2)}) async-start(bf16[128,4,256]{0,2,1:T(8,128)(2,1)} %bitcast.26), calls=%async_computation.3 | async-start | bytes 524288 | tf_op jit(solution)/shard_map/all_to_all | solution.py:109
  34.3 2.1 %copy.46 = bf16[1,128,2048]{1,2,0:T(8,128)(2,1)} copy(bf16[1,128,2048]{2,1,0:T(8,128)(2,1)} %param.11) | data formatting | bytes 1048576 | tf_op args[2]
  36.4 4.7 %all-to-all-done.3 = bf16[128,4,256]{0,2,1:T(8,128)(2,1)S(1)} async-done(((bf16[128,4,256]{0,2,1:T(8,128)(2,1)}), bf16[128,4,256]{0,2,1:T(8,128)(2,1)S(1)}, u32[]{:S(2)}, u32[]{:S(2)}) %all-to-all-start.3) | async-done | bytes 262176 | tf_op jit(solution)/shard_map/all_to_all | solution.py:109
  41.1 3.5 %all-to-all-start.2 = ((bf16[128,4,512]{0,2,1:T(8,128)(2,1)}), bf16[128,4,512]{0,2,1:T(8,128)(2,1)S(1)}, u32[]{:S(2)}, u32[]{:S(2)}) async-start(bf16[128,4,512]{0,2,1:T(8,128)(2,1)} %bitcast.22), calls=%async_computation.2 | async-start | bytes 1048576 | tf_op jit(solution)/shard_map/all_to_all | solution.py:113
  44.6 0.8 fusion.58
  45.4 3.7 %collective-permute-start.2 = (bf16[128,1]{0,1:T(2,128)(2,1)S(1)}, bf16[128,1]{0,1:T(2,128)(2,1)S(1)}, u32[]{:S(2)}, u32[]{:S(2)}) collective-permute-start(bf16[128,1]{0,1:T(2,128)(2,1)S(1)} %get-tuple-element.161), channel_id=1, source_target_pairs={{0,24},{8,0},{16,8},{24,16},{1,25},{9,1},{17,9},{25,17},{2,26},{10... | collective-permute-start | bytes 776 | tf_op jit(solution)/shard_map/ppermute | solution.py:27
  49.2 1.1 collective-permute-start.1
  50.5 4.1 %collective-permute-done = bf16[128,1]{0,1:T(2,128)(2,1)S(1)} collective-permute-done((bf16[128,1]{0,1:T(2,128)(2,1)S(1)}, bf16[128,1]{0,1:T(2,128)(2,1)S(1)}, u32[]{:S(2)}, u32[]{:S(2)}) %collective-permute-start) | collective-permute-done | bytes 288 | tf_op jit(solution)/shard_map/ppermute | solution.py:27
  54.5 0.8 collective-permute-done.1
  56.0 31.5 %while.17 = (s32[]{:T(128)}, f32[256,512]{1,0:T(8,128)S(1)}, f32[256]{0:T(256)S(1)}, f32[]{:T(128)}, bf16[4,128,512]{1,2,0:T(8,128)(2,1)}, /*index=5*/f32[4,128]...) while((s32[]{:T(128)}, f32[256,512]{1,0:T(8,128)S(1)}, ...), condition=%wide.region_5.6_spmd.clone, body=%wide.region_0.5_spmd.clone.sunk | while | flops 555633152 | bytes 3825425 | solution.py:86
  56.9 0.7 subtract_reduce_fusion.2
  57.6 1.3 %fusion.99 = (f32[]{:T(128)}, f32[128]{0:T(128)S(1)}) fusion(f32[128]{0:T(128)S(1)} %get-tuple-element.235, f32[]{:T(128)} %bitcast.157, f32[4,128]{1,0:T(4,128)S(1)} %get-tuple-element.278, s32[]{:T(128)} %get-tuple-element.259), kind=kLoop, calls=%fused_computation.64.clone.1 | loop fusion | flops 383 | bytes 1548 | tf_op jit(solution)/shard_map/while/body/eval_jaxpr/reduce_max | solution.py:66
  62.6 0.7 constant_dynamic-update-slice_fusion.2
  64.7 0.7 subtract_reduce_fusion.2
  65.5 1.3 %fusion.99 = (f32[]{:T(128)}, f32[128]{0:T(128)S(1)}) fusion(f32[128]{0:T(128)S(1)} %get-tuple-element.235, f32[]{:T(128)} %bitcast.157, f32[4,128]{1,0:T(4,128)S(1)} %get-tuple-element.278, s32[]{:T(128)} %get-tuple-element.259), kind=kLoop, calls=%fused_computation.64.clone.1 | loop fusion | flops 383 | bytes 1548 | tf_op jit(solution)/shard_map/while/body/eval_jaxpr/reduce_max | solution.py:66
  70.5 0.7 constant_dynamic-update-slice_fusion.2
  72.6 0.7 subtract_reduce_fusion.2
  73.4 1.3 %fusion.99 = (f32[]{:T(128)}, f32[128]{0:T(128)S(1)}) fusion(f32[128]{0:T(128)S(1)} %get-tuple-element.235, f32[]{:T(128)} %bitcast.157, f32[4,128]{1,0:T(4,128)S(1)} %get-tuple-element.278, s32[]{:T(128)} %get-tuple-element.259), kind=kLoop, calls=%fused_computation.64.clone.1 | loop fusion | flops 383 | bytes 1548 | tf_op jit(solution)/shard_map/while/body/eval_jaxpr/reduce_max | solution.py:66
  80.5 0.7 subtract_reduce_fusion.2
  81.3 1.3 %fusion.99 = (f32[]{:T(128)}, f32[128]{0:T(128)S(1)}) fusion(f32[128]{0:T(128)S(1)} %get-tuple-element.235, f32[]{:T(128)} %bitcast.157, f32[4,128]{1,0:T(4,128)S(1)} %get-tuple-element.278, s32[]{:T(128)} %get-tuple-element.259), kind=kLoop, calls=%fused_computation.64.clone.1 | loop fusion | flops 383 | bytes 1548 | tf_op jit(solution)/shard_map/while/body/eval_jaxpr/reduce_max | solution.py:66
  86.3 0.7 constant_dynamic-update-slice_fusion.2
  87.6 3.5 %all-to-all-start.4 = ((bf16[4,128,512]{1,2,0:T(8,128)(2,1)}), bf16[4,128,512]{1,2,0:T(8,128)(2,1)S(1)}, u32[]{:S(2)}, u32[]{:S(2)}) async-start(bf16[4,128,512]{1,2,0:T(8,128)(2,1)} %get-tuple-element.62), calls=%async_computation.4 | async-start | bytes 1048576 | tf_op jit(solution)/shard_map/all_to_all | solution.py:131
  91.3 10.0 %all-to-all-done.4 = bf16[4,128,512]{1,2,0:T(8,128)(2,1)S(1)} async-done(((bf16[4,128,512]{1,2,0:T(8,128)(2,1)}), bf16[4,128,512]{1,2,0:T(8,128)(2,1)S(1)}, u32[]{:S(2)}, u32[]{:S(2)}) %all-to-all-start.4) | async-done | bytes 524320 | tf_op jit(solution)/shard_map/all_to_all | solution.py:131
  101.6 5.5 %fusion.49 = bf16[1,128,2048]{2,1,0:T(8,128)(2,1)} fusion(bf16[128,2048]{0,1:T(8,128)(2,1)S(1)} %fusion.50, bf16[2048,2048]{1,0:T(8,128)(2,1)} %all-gather.2.cloned.1.call-done), kind=kOutput, calls=%fused_computation.66 | convolution fusion | flops 1074003968 | bytes 9437184 | tf_op jit(solution)/shard_map/dot_general | solution.py:135
  (83 shorter events, 16.8 us)
Async XLA Ops:
  6.5 95.1 %all-gather.2.cloned.1.call-start = ((), (), s32[]{:S(2)}) async-start(), calls=%async_computation.5 | async-start | bytes 9437184 | tf_op jit(solution)/shard_map/all_gather | solution.py:137
  8.5 11.9 %all-to-all-start = ((bf16[128,4,1]{0,2,1:T(2,128)(2,1)}), bf16[128,4,1]{0,2,1:T(2,128)(2,1)S(1)}, u32[]{:S(2)}, u32[]{:S(2)}) async-start(bf16[128,4,1]{0,2,1:T(2,128)(2,1)} %copy.44), calls=%async_computation | async-start | bytes 4096 | tf_op jit(solution)/shard_map/all_to_all | solution.py:120
  20.4 10.5 %all-to-all-start.1 = ((bf16[128,4,256]{0,2,1:T(8,128)(2,1)}), bf16[128,4,256]{0,2,1:T(8,128)(2,1)S(1)}, u32[]{:S(2)}, u32[]{:S(2)}) async-start(bf16[128,4,256]{0,2,1:T(8,128)(2,1)} %bitcast.18), calls=%async_computation.1 | async-start | bytes 524288 | tf_op jit(solution)/shard_map/all_to_all | solution.py:110
  30.9 10.2 %all-to-all-start.3 = ((bf16[128,4,256]{0,2,1:T(8,128)(2,1)}), bf16[128,4,256]{0,2,1:T(8,128)(2,1)S(1)}, u32[]{:S(2)}, u32[]{:S(2)}) async-start(bf16[128,4,256]{0,2,1:T(8,128)(2,1)} %bitcast.26), calls=%async_computation.3 | async-start | bytes 524288 | tf_op jit(solution)/shard_map/all_to_all | solution.py:109
  41.1 14.9 %all-to-all-start.2 = ((bf16[128,4,512]{0,2,1:T(8,128)(2,1)}), bf16[128,4,512]{0,2,1:T(8,128)(2,1)S(1)}, u32[]{:S(2)}, u32[]{:S(2)}) async-start(bf16[128,4,512]{0,2,1:T(8,128)(2,1)} %bitcast.22), calls=%async_computation.2 | async-start | bytes 1048576 | tf_op jit(solution)/shard_map/all_to_all | solution.py:113
  45.4 5.0 %collective-permute-start.2 = (bf16[128,1]{0,1:T(2,128)(2,1)S(1)}, bf16[128,1]{0,1:T(2,128)(2,1)S(1)}, u32[]{:S(2)}, u32[]{:S(2)}) collective-permute-start(bf16[128,1]{0,1:T(2,128)(2,1)S(1)} %get-tuple-element.161), channel_id=1, source_target_pairs={{0,24},{8,0},{16,8},{24,16},{1,25},{9,1},{17,9},{25,17},{2,26},{10... | collective-permute-start | bytes 776 | tf_op jit(solution)/shard_map/ppermute | solution.py:27
  49.2 5.4 %collective-permute-start = (bf16[128,1]{0,1:T(2,128)(2,1)S(1)}, bf16[128,1]{0,1:T(2,128)(2,1)S(1)}, u32[]{:S(2)}, u32[]{:S(2)}) collective-permute-start(bf16[128,1]{0,1:T(2,128)(2,1)S(1)} %get-tuple-element.160), channel_id=1, source_target_pairs={{0,8},{8,16},{16,24},{24,0},{1,9},{9,17},{17,25},{25,1},{2,10},{10... | collective-permute-start | bytes 776 | tf_op jit(solution)/shard_map/ppermute | solution.py:27
  49.2 6.2 %collective-permute-start.1 = (bf16[128,1]{0,1:T(2,128)(2,1)S(1)}, bf16[128,1]{0,1:T(2,128)(2,1)S(1)}, u32[]{:S(2)}, u32[]{:S(2)}) collective-permute-start(bf16[128,1]{0,1:T(2,128)(2,1)S(1)} %get-tuple-element.162), channel_id=1, source_target_pairs={{0,16},{8,24},{16,0},{24,8},{1,17},{9,25},{17,1},{25,9},{2,18},{10... | collective-permute-start | bytes 776 | tf_op jit(solution)/shard_map/ppermute | solution.py:27
  56.0 35.0 %copy-start = (bf16[1,128,2048]{2,1,0:T(8,128)(2,1)S(1)}, bf16[1,128,2048]{2,1,0:T(8,128)(2,1)}, u32[]{:S(2)}) copy-start(bf16[1,128,2048]{2,1,0:T(8,128)(2,1)} %param.12) | copy-start | bytes 1572868
  87.6 13.7 %all-to-all-start.4 = ((bf16[4,128,512]{1,2,0:T(8,128)(2,1)}), bf16[4,128,512]{1,2,0:T(8,128)(2,1)S(1)}, u32[]{:S(2)}, u32[]{:S(2)}) async-start(bf16[4,128,512]{1,2,0:T(8,128)(2,1)} %get-tuple-element.62), calls=%async_computation.4 | async-start | bytes 1048576 | tf_op jit(solution)/shard_map/all_to_all | solution.py:131
Sparse Core Ops, SparseCore 0:
  9.2 58.5 all-gather.1
